TPU v7x, 32 devices: a whole 2x2x4 slice. The times are simulated.
32 devices in a mesh: kv: 8 (over z, x), tp: 4 (over y, core).
Axes of the slice: x: 2, y: 2, z: 4, core: 2. Of those that a mesh axis runs over, the one named last changes fastest.
Arguments:
- tokens: bfloat16 [32, 2048], P(None, 'kv'), may hold values from -6 to 6
- token_gain: float32 [2048], P('kv'), may hold values from 0.1 to 1.9
- w_query: bfloat16 [2048, 1536], P('kv', 'tp'), may hold values from -0.125 to 0.125
- w_down_kv: bfloat16 [2048, 512], P('kv'), may hold values from -0.125 to 0.125
- w_rope_key: bfloat16 [2048, 64], P('kv'), may hold values from -0.125 to 0.125
- latent_gain: float32 [512], replicated, may hold values from 0.1 to 1.9
- w_key_up: bfloat16 [8, 512, 128], P('tp'), may hold values from -0.25 to 0.25
- w_value_up: bfloat16 [8, 512, 128], P('tp'), may hold values from -0.25 to 0.25
- w_out: bfloat16 [1024, 2048], P('tp', 'kv'), may hold values from -0.1875 to 0.1875
- out_gain: float32 [2048], P('kv'), may hold values from 0.1 to 1.9
- cache_latent: bfloat16 [32, 4096, 512], P('tp', 'kv'), may hold values from -6 to 6
- cache_rope: bfloat16 [32, 4096, 64], P('tp', 'kv'), may hold values from -6 to 6
- lengths: int32 [32], replicated, may hold values from 1 to 4095, as said below
Outputs:
- mixed: bfloat16 [32, 2048], P(None, 'kv')
Inputs may be any that keep to these rules, and one draw needn't show every extreme that they name: `lengths`: each of the 32 sequences has 1 to 4095 cached positions; some sequence has exactly 4095 and some exactly 1.
All inputs are finite; a program needn't handle non-finite values.
Results may differ from a plain program's by a relative error of at most 0.015.
Values may be sent and summed in bfloat16 or wider, within the bound.
A program may use at most 64 MiB of HBM per device.

v0:
```python
import jax
import jax.numpy as jnp
from jax import lax
from jax.sharding import PartitionSpec as P

EPSILON = 1e-06
NEGATIVE = -1e30


def joined_2(part, axis, combine):
    gathered = jax.tree.map(lambda a: lax.all_gather(a, axis), part)

    def take(source):
        return jax.tree.map(lambda a: lax.dynamic_index_in_dim(a, source, 0, False), gathered)

    return lax.fori_loop(
        1, lax.axis_size(axis), lambda source, state: combine(state, take(source)), take(0)
    )


def rotate_half(values, cosine, sine_table):
    half_width = values.shape[-1] // 2
    lower_half = values[..., :half_width]
    upper_half = values[..., half_width:]
    return jnp.concatenate(
        [
            lower_half * cosine - upper_half * sine_table,
            upper_half * cosine + lower_half * sine_table,
        ],
        axis=-1,
    )


def angle_tables(lengths, rope_width):
    inverse_freq = 1.0 / 10000.0 ** (jnp.arange(0, rope_width, 2, dtype=jnp.float32) / rope_width)
    angles = lengths.astype(jnp.float32)[:, None] * inverse_freq[None, :]
    return (jnp.cos(angles), jnp.sin(angles))


def combine_parts(earlier, later):
    first_max, first_sum, first_acc = earlier
    second_max, second_sum, second_acc = later
    joined = jnp.maximum(first_max, second_max)
    first_fac = jnp.exp(first_max - joined)
    second_fac = jnp.exp(second_max - joined)
    return (
        joined,
        first_sum * first_fac + second_sum * second_fac,
        first_acc * first_fac[..., None] + second_acc * second_fac[..., None],
    )


def on_device(
    tokens,
    token_gain,
    w_query,
    w_down_kv,
    w_rope_key,
    latent_gain,
    w_key_up,
    w_value_up,
    w_out,
    out_gain,
    cache_latent,
    cache_rope,
    lengths,
):
    model_width = tokens.shape[1] * lax.axis_size("kv")
    seq_count = tokens.shape[0]
    local_heads, latent_width, nope_width = w_key_up.shape
    rope_width = w_rope_key.shape[1]
    head_width = nope_width + rope_width
    factor = head_width ** (-0.5)
    token_values = tokens.astype(jnp.float32)
    scaled = (token_values * token_gain).astype(jnp.bfloat16)
    query_part = jnp.dot(scaled, w_query, preferred_element_type=jnp.float32)
    latent_part = jnp.dot(scaled, w_down_kv, preferred_element_type=jnp.float32)
    rope_part = jnp.dot(scaled, w_rope_key, preferred_element_type=jnp.float32)
    query_raw, latent_raw, rope_raw = lax.psum((query_part, latent_part, rope_part), "kv")
    query_heads = query_raw.astype(jnp.bfloat16).reshape(seq_count, local_heads, head_width)
    latent = (
        latent_raw
        * lax.rsqrt(jnp.mean(latent_raw * latent_raw, axis=1, keepdims=True) + EPSILON)
        * latent_gain
    ).astype(jnp.bfloat16)
    cosine, sine_table = angle_tables(lengths, rope_width)
    new_rope = rotate_half(rope_raw, cosine, sine_table).astype(jnp.bfloat16)
    query_nope = query_heads[..., :nope_width]
    query_rope = rotate_half(
        query_heads[..., nope_width:].astype(jnp.float32),
        cosine[:, None, :],
        sine_table[:, None, :],
    ).astype(jnp.bfloat16)
    query_latent = jnp.einsum(
        "bhn,hcn->bhc", query_nope, w_key_up, preferred_element_type=jnp.float32
    ).astype(jnp.bfloat16)
    seq_latent, seq_rope = (
        lax.all_to_all(query_latent, "tp", split_axis=0, concat_axis=1, tiled=True),
        lax.all_to_all(query_rope, "tp", split_axis=0, concat_axis=1, tiled=True),
    )
    local_seqs = cache_latent.shape[0]
    local_pos = cache_latent.shape[1]
    first_row = lax.axis_index("tp") * local_seqs
    own_latent = lax.dynamic_slice_in_dim(latent, first_row, local_seqs, 0)
    own_rope = lax.dynamic_slice_in_dim(new_rope, first_row, local_seqs, 0)
    own_length = lax.dynamic_slice_in_dim(lengths, first_row, local_seqs, 0)
    first_pos = lax.axis_index("kv") * local_pos
    positions = first_pos + jnp.arange(local_pos, dtype=jnp.int32)
    scores = (
        jnp.einsum("bhc,blc->bhl", seq_latent, cache_latent, preferred_element_type=jnp.float32)
        + jnp.einsum("bhr,blr->bhl", seq_rope, cache_rope, preferred_element_type=jnp.float32)
    ) * factor
    visible = positions[None, None, :] < own_length[:, None, None]
    new_score = (
        jnp.einsum("bhc,bc->bh", seq_latent, own_latent, preferred_element_type=jnp.float32)
        + jnp.einsum("bhr,br->bh", seq_rope, own_rope, preferred_element_type=jnp.float32)
    ) * factor
    holder = ((own_length >= first_pos) & (own_length < first_pos + local_pos))[:, None]
    local_max = jnp.maximum(
        jnp.max(jnp.where(visible, scores, NEGATIVE), axis=2),
        jnp.where(holder, new_score, NEGATIVE),
    )
    weights = jnp.where(visible, jnp.exp(scores - local_max[..., None]), 0.0)
    new_weight = jnp.where(holder, jnp.exp(new_score - local_max), 0.0)
    weight_sum = jnp.sum(weights, axis=2) + new_weight
    rounded_new = lax.optimization_barrier(new_weight.astype(jnp.bfloat16)).astype(jnp.float32)
    weighted = (
        jnp.einsum(
            "bhl,blc->bhc",
            weights.astype(jnp.bfloat16),
            cache_latent,
            preferred_element_type=jnp.float32,
        )
        + rounded_new[..., None] * own_latent.astype(jnp.float32)[:, None, :]
    )
    local_max, weight_sum, weighted = joined_2(
        (local_max, weight_sum, weighted), "kv", combine_parts
    )
    head_latent = (weighted / weight_sum[..., None]).astype(jnp.bfloat16)
    batch_latent = lax.all_to_all(head_latent, "tp", split_axis=1, concat_axis=0, tiled=True)
    head_out = (
        jnp.einsum("bhc,hcv->bhv", batch_latent, w_value_up, preferred_element_type=jnp.float32)
        .astype(jnp.bfloat16)
        .reshape(seq_count, -1)
    )
    mixed_sum = lax.psum(jnp.dot(head_out, w_out, preferred_element_type=jnp.float32), "tp")
    out_squares = lax.psum(jnp.sum(mixed_sum * mixed_sum, axis=1), "kv")
    return (mixed_sum * lax.rsqrt(out_squares / model_width + EPSILON)[:, None] * out_gain).astype(
        jnp.bfloat16
    )


def solution(mesh):
    placed = (
        P(None, "kv"),
        P("kv"),
        P("kv", "tp"),
        P("kv", None),
        P("kv", None),
        P(),
        P("tp", None, None),
        P("tp", None, None),
        P("tp", "kv"),
        P("kv"),
        P("tp", "kv", None),
        P("tp", "kv", None),
        P(),
    )
    return jax.shard_map(
        on_device, mesh=mesh, in_specs=placed, out_specs=P(None, "kv"), check_vma=False
    )
```

profile of v0, /device:TPU:0, one launch (start us, length us, event | category | flops | bytes accessed | tf_op | source)
XLA Modules:
  0.0 245.0 jit_solution(3555207810225279691)
XLA Ops:
  6.5 0.0 copy-start
  6.5 0.0 copy-start.3
  6.5 0.7 convert_element_type.56
  7.3 0.9 fusion.23
  8.2 1.1 fusion.25
  9.3 39.4 %all-reduce = (bf16[32,384]{1,0:T(8,128)(2,1)S(1)}, f32[32,64]{1,0:T(8,128)S(1)}) all-reduce(f32[32,384]{1,0:T(8,128)S(1)} %fusion.25, f32[32,64]{1,0:T(8,128)S(1)} %fusion.23), channel_id=1, replica_groups=mesh['kv'=8,'tp'=4] {'kv'}, use_global_device_ids=true, to_apply=%region_0.0 | all-reduce | flops 14336 | bytes 90112 | tf_op jit(solution)/shard_map/psum | solution.py:79
  48.7 0.1 reshape.109
  48.8 0.1 add_convert_fusion.1
  48.9 0.1 subtract_convert_fusion
  49.0 0.1 pad_maximum_fusion
  49.1 0.7 reshape.124
  49.8 3.2 %all-to-all-start.1 = ((bf16[4,2,512]{2,1,0:T(2,128)(2,1)}), bf16[4,2,512]{2,1,0:T(2,128)(2,1)S(1)}, u32[]{:S(2)}, u32[]{:S(2)}) async-start(bf16[4,2,512]{2,1,0:T(2,128)(2,1)} %reshape.124), calls=%async_computation.1 | async-start | bytes 16384 | tf_op jit(solution)/shard_map/all_to_all | solution.py:99
  53.1 0.0 all-reduce.3.cloned.1.call-start
  53.1 1.8 fusion.24
  54.9 0.0 all-reduce.3.cloned.1.call-update
  55.0 0.7 compare_and_fusion
  55.7 0.1 broadcast_compare_fusion
  55.8 1.1 fusion.4
  56.9 0.1 fusion.29
  57.0 0.7 copy.24
  57.7 0.0 all-to-all-done.1
  57.7 3.3 %all-to-all-start = ((bf16[32,2,512]{2,1,0:T(2,128)(2,1)}), bf16[32,2,512]{2,1,0:T(2,128)(2,1)S(1)}, u32[]{:S(2)}, u32[]{:S(2)}) async-start(bf16[32,2,512]{2,1,0:T(2,128)(2,1)} %copy.24), calls=%async_computation | async-start | bytes 131072 | tf_op jit(solution)/shard_map/all_to_all | solution.py:98
  61.0 0.0 all-gather.5.cloned.1.call-start
  61.0 0.1 reshape.125
  61.2 0.1 fusion.26
  61.3 3.8 %all-to-all-done = bf16[32,2,512]{2,1,0:T(2,128)(2,1)S(1)} async-done(((bf16[32,2,512]{2,1,0:T(2,128)(2,1)}), bf16[32,2,512]{2,1,0:T(2,128)(2,1)S(1)}, u32[]{:S(2)}, u32[]{:S(2)}) %all-to-all-start) | async-done | bytes 65568 | tf_op jit(solution)/shard_map/all_to_all | solution.py:98
  65.2 3.4 %fusion.35 = f32[8,8,512]{2,1,0:T(8,128)S(1)} fusion(bf16[8,8,512]{2,1,0:T(8,128)(2,1)S(1)} %all_to_all.42, bf16[8,512,512]{2,1,0:T(8,128)(2,1)} %param.25), kind=kOutput, calls=%fused_computation.70 | convolution fusion | flops 33554432 | bytes 4390912 | tf_op jit(solution)/shard_map/bhc,blc->bhl/dot_general | solution.py:110
  68.5 0.0 copy-done
  68.5 0.3 select_reduce_fusion
  68.8 0.0 copy-start.1
  68.8 55.9 %all-reduce.3.cloned.1.call-done = f32[32,512]{1,0:T(8,128)} async-done(((f32[32,512]{1,0:T(8,128)}), f32[32,512]{1,0:T(8,128)}) %all-reduce.3.cloned.1.call-update) | async-done | bytes 65552 | tf_op jit(solution)/shard_map/psum | solution.py:79
  124.7 1.0 multiply_reduce_fusion
  125.7 0.1 dynamic-slice
  125.7 0.0 copy-done.3
  125.7 0.8 fusion.32
  126.5 0.1 fusion.21
  126.7 0.1 fusion.34
  126.8 0.0 copy-start.4
  126.8 3.6 %convolution_add_fusion.1 = f32[8,8,512]{2,1,0:T(8,128)} fusion(bf16[8,512,512]{2,1,0:T(8,128)(2,1)} %param.25, f32[8,8,512]{2,1,0:T(8,128)S(1)} %get-tuple-element.218, f32[8,512]{1,0:T(8,128)S(1)} %get-tuple-element.208, f32[8,8]{1,0:T(8,128)S(1)} %convert_element_type.60, f32[8,8]{1,0:T(8,128)S(1)} %get-tuple-element.214, ...), kind=kOutput, calls=%fused_computation.10 | convolution fusion | flops 33718272 | bytes 4477440 | tf_op jit(solution)/shard_map/bhl,blc->bhc/dot_general | solution.py:128
  130.3 0.0 all-gather.5.cloned.1.call-update
  130.4 0.2 fusion.8
  130.5 30.6 %all-gather.1 = f32[64,8]{1,0:T(8,128)S(1)} all-gather(f32[8,8]{1,0:T(8,128)S(1)} %add.131), channel_id=3, replica_groups=mesh['kv'=8,'tp'=4] {'kv'}, dimensions={0}, use_global_device_ids=true | all-gather | bytes 2304 | tf_op jit(solution)/shard_map/all_gather | solution.py:11
  161.1 30.5 %all-gather = f32[64,8]{1,0:T(8,128)S(1)} all-gather(f32[8,8]{1,0:T(8,128)S(1)} %get-tuple-element.214), channel_id=2, replica_groups=mesh['kv'=8,'tp'=4] {'kv'}, dimensions={0}, use_global_device_ids=true | all-gather | bytes 2304 | tf_op jit(solution)/shard_map/all_gather | solution.py:11
  191.6 0.9 slice.38
  192.5 7.3 %while.19 = (s32[]{:T(128)}, f32[8,8]{1,0:T(8,128)S(1)}, f32[8,8]{1,0:T(8,128)S(1)}, f32[8,8,512]{2,1,0:T(8,128)S(1)}, f32[8,8,8]{2,1,0:T(8,128)S(1)}, /*index=5...) while((s32[]{:T(128)}, f32[8,8]{1,0:T(8,128)S(1)}, ...), condition=%wide.region_7.8_spmd, body=%wide.region_6.7_spmd.sunk | while | flops 98693 | bytes 395919 | solution.py:16
  192.6 1.0 fusion.52
  193.6 1.0 fusion.52
  194.7 1.0 fusion.52
  195.7 1.0 fusion.52
  196.8 1.0 fusion.52
  197.8 1.0 fusion.52
  198.9 1.0 fusion.52
  199.9 0.1 copy.27
  200.0 0.1 fusion.6
  200.1 6.7 %all_to_all.54 = bf16[8,8,512]{2,0,1:T(8,128)(2,1)S(1)} all-to-all(bf16[8,8,512]{2,0,1:T(8,128)(2,1)S(1)} %fusion.6), channel_id=1, replica_groups=mesh['kv'=8,'tp'=4] {'tp'}, dimensions={1} | all-to-all | bytes 131072 | tf_op jit(solution)/shard_map/all_to_all | solution.py:140
  206.7 0.0 copy-done.1
  206.7 0.2 fusion.5
  206.9 0.0 copy-done.2
  206.9 0.1 fusion.15
  207.0 10.3 %psum.38 = f32[32,256]{1,0:T(8,128)S(1)} all-reduce(f32[32,256]{1,0:T(8,128)S(1)} %fusion.15), channel_id=1, replica_groups=mesh['kv'=8,'tp'=4] {'tp'}, use_global_device_ids=true, to_apply=%region_8.9 | all-reduce | flops 8192 | bytes 65536 | tf_op jit(solution)/shard_map/psum | solution.py:146
  217.3 0.1 multiply_reduce_fusion.1
  217.4 20.1 %psum.39 = f32[32]{0:T(128)S(1)} all-reduce(f32[32]{0:T(128)S(1)} %multiply_reduce_fusion.1), channel_id=1, replica_groups=mesh['kv'=8,'tp'=4] {'kv'}, use_global_device_ids=true, to_apply=%region_10.11 | all-reduce | flops 32 | bytes 256 | tf_op jit(solution)/shard_map/psum | solution.py:147
  237.5 0.0 copy-done.4
  237.5 0.7 multiply_convert_fusion
  (22 shorter events, 0.3 us)
Async XLA Ops:
  6.5 62.0 %copy-start = (bf16[8,512,64]{1,2,0:T(8,128)(2,1)S(1)}, bf16[8,512,64]{1,2,0:T(8,128)(2,1)}, u32[]{:S(2)}) copy-start(bf16[8,512,64]{1,2,0:T(8,128)(2,1)} %param.26) | copy-start | bytes 1572868
  6.5 119.2 %copy-start.3 = (f32[512]{0:T(512)S(1)}, f32[512]{0:T(512)}, u32[]{:S(2)}) copy-start(f32[512]{0:T(512)} %param.20) | copy-start | bytes 6148
  49.8 7.9 %all-to-all-start.1 = ((bf16[4,2,512]{2,1,0:T(2,128)(2,1)}), bf16[4,2,512]{2,1,0:T(2,128)(2,1)S(1)}, u32[]{:S(2)}, u32[]{:S(2)}) async-start(bf16[4,2,512]{2,1,0:T(2,128)(2,1)} %reshape.124), calls=%async_computation.1 | async-start | bytes 16384 | tf_op jit(solution)/shard_map/all_to_all | solution.py:99
  53.1 71.6 %all-reduce.3.cloned.1.call-start = ((), (), s32[]{:S(2)}) async-start(), calls=%async_computation.3 | async-start | bytes 131072 | tf_op jit(solution)/shard_map/psum | solution.py:79
  57.7 7.4 %all-to-all-start = ((bf16[32,2,512]{2,1,0:T(2,128)(2,1)}), bf16[32,2,512]{2,1,0:T(2,128)(2,1)S(1)}, u32[]{:S(2)}, u32[]{:S(2)}) async-start(bf16[32,2,512]{2,1,0:T(2,128)(2,1)} %copy.24), calls=%async_computation | async-start | bytes 131072 | tf_op jit(solution)/shard_map/all_to_all | solution.py:98
  61.0 130.6 %all-gather.5.cloned.1.call-start = ((), (), s32[]{:S(2)}) async-start(), calls=%async_computation.4 | async-start | bytes 1179648 | tf_op jit(solution)/shard_map/all_gather | solution.py:11
  68.8 137.9 %copy-start.1 = (bf16[2,512,128]{2,1,0:T(8,128)(2,1)S(1)}, bf16[2,512,128]{2,1,0:T(8,128)(2,1)}, u32[]{:S(2)}) copy-start(bf16[2,512,128]{2,1,0:T(8,128)(2,1)} %param.22) | copy-start | bytes 786436
  126.5 80.4 %copy-start.2 = (bf16[256,256]{1,0:T(8,128)(2,1)S(1)}, bf16[256,256]{1,0:T(8,128)(2,1)}, u32[]{:S(2)}) copy-start(bf16[256,256]{1,0:T(8,128)(2,1)} %param.23) | copy-start | bytes 393220
  126.8 110.7 %copy-start.4 = (f32[256]{0:T(256)S(1)}, f32[256]{0:T(256)}, u32[]{:S(2)}) copy-start(f32[256]{0:T(256)} %param.24) | copy-start | bytes 3076
Sparse Core Ops, SparseCore 0:
  57.3 67.3 all-reduce.2
  130.5 40.4 all-gather.4
where the time goes:
time: 246 us; the launch traced here: 245 us
  blocking collectives  137 us (56%)
  waiting for transfers between devices  59.7 us (24%)
  between operations  13.6 us (6%)
  matrix products  12.6 us (5%)
  other arithmetic  12 us (5%)
  starting transfers between devices  6.61 us (3%)
  local copies, waits for them, and re-layouts  2.78 us (1%)
    all_gather x2, blocking collectives, joined_2(): gathered = jax.tree.map(lambda a: lax.all_gather(a, axis), part)  61.1 us
    psum x1, waiting for transfers between devices, on_device(): lax.psum((query_part, latent_part, rope_part), 'kv')  55.9 us
    psum x1, blocking collectives, on_device(): lax.psum((query_part, latent_part, rope_part), 'kv')  39.4 us
    psum x1, blocking collectives, on_device(): out_squares = lax.psum(jnp.sum(mixed_sum * mixed_sum, axis=1), 'kv')  20.1 us
    psum x1, blocking collectives, on_device(): lax.psum(jnp.dot(head_out, w_out, preferred_element_type=jnp.float32), 'tp')  10.3 us
    add x7, other arithmetic, combine_parts(): first_acc * first_fac[..., None] + second_acc * second_fac[..., None]  7 us
    all_to_all x1, blocking collectives, on_device(): lax.all_to_all(head_latent, 'tp', split_axis=1, concat_axis=0, tiled=True)  6.67 us
  transfers between devices with their start and end apart: 4, of which 2 were waited for; matrix products, arithmetic and copies ran while one was open for 4% of the time, Pallas kernels for 0%

commit v1 on v0

v1 whole, which is shorter than its diff:
```python
import functools

import jax
import jax.numpy as jnp
from jax import lax
from jax.experimental import pallas as pl
from jax.experimental.pallas import tpu as pltpu
from jax.sharding import PartitionSpec as P

EPSILON = 1e-06
NEGATIVE = -1e30
LANES = 128
MESH = pl.DeviceIdType.MESH
F32 = jnp.float32
BF16 = jnp.bfloat16


def rounded(values):
    return values.astype(BF16).astype(F32)


def rotated(values, cosine, signed_sine, half):
    lane = lax.broadcasted_iota(jnp.int32, values.shape, 1)
    swapped = jnp.where(
        lane < half, pltpu.roll(values, LANES - half, 1), pltpu.roll(values, half, 1)
    )
    return values * cosine + swapped * signed_sine


def dot_t(a, b):
    return lax.dot_general(a, b, (((1,), (1,)), ((), ())), preferred_element_type=F32)


def kernel(
    kv,
    tp,
    lengths,
    tok_h,
    tgain_h,
    wq_h,
    wd_h,
    wr_h,
    cos_h,
    sin_h,
    wku_h,
    cl_h,
    cr_h,
    lgain_h,
    wvu_h,
    wo_h,
    ogain_h,
    out,
    tok,
    tgain,
    wq,
    wd,
    wr,
    cos,
    sin,
    wku,
    cl,
    cr,
    lgain,
    wvu,
    wo,
    ogain,
    scaled_s,
    q_send,
    q_recv,
    lat_send,
    lat_recv,
    row_send,
    row_recv,
    ql_send,
    ql_recv,
    q32,
    stage,
    part_send,
    part_recv,
    hl_send,
    hl_recv,
    mix_send,
    mix_recv,
    sq_send,
    sq_recv,
    in_sem,
    q_ss,
    q_rs,
    lat_ss,
    lat_rs,
    row_ss,
    row_rs,
    ql_ss,
    ql_rs,
    part_ss,
    part_rs,
    hl_ss,
    hl_rs,
    mix_ss,
    mix_rs,
    sq_ss,
    sq_rs,
):
    k = lax.axis_index("kv")
    t = lax.axis_index("tp")
    batch, width = tok.shape
    lh, latent, nope_w = wku.shape
    rope_w = wr.shape[1]
    head_w = nope_w + rope_w
    half = rope_w // 2
    factor = head_w ** (-0.5)
    seqs, pos = cl.shape[0], cl.shape[1]
    heads = lh * tp
    full = latent + LANES
    per_row = kv // tp
    dup = per_row // lh
    lat_dup = kv // seqs
    rows = heads * seqs // kv
    parts = seqs // rows
    model_w = width * kv
    chunk = q_send.shape[2]

    loads = [
        pltpu.make_async_copy(a, b, in_sem.at[i])
        for i, (a, b) in enumerate(
            [
                (tok_h, tok),
                (tgain_h, tgain),
                (wq_h, wq),
                (wd_h, wd),
                (wr_h, wr),
                (cos_h, cos),
                (sin_h, sin),
                (wku_h, wku),
                (lgain_h, lgain),
                (cl_h, cl),
                (cr_h, cr),
                (wvu_h, wvu),
                (wo_h, wo),
                (ogain_h, ogain),
            ]
        )
    ]
    for load in loads:
        load.start()

    barrier = pltpu.get_barrier_semaphore()
    me = k * tp + t

    def greet(i, carry):
        @pl.when(i != me)
        def _():
            pl.semaphore_signal(
                barrier, inc=1, device_id=(i // tp, i % tp), device_id_type=MESH
            )

        return carry

    lax.fori_loop(0, kv * tp, greet, 0)

    def remote(src, dst, send, recv, kk, tt):
        return pltpu.make_async_remote_copy(
            src_ref=src,
            dst_ref=dst,
            send_sem=send,
            recv_sem=recv,
            device_id=(kk, tt),
            device_id_type=MESH,
        )

    def push(src, dst, send, recv, kk, tt):
        same = jnp.logical_and(kk == k, tt == t)

        @pl.when(jnp.logical_not(same))
        def _():
            remote(src, dst, send, recv, kk, tt).start()

        @pl.when(same)
        def _():
            pltpu.make_async_copy(src, dst, recv).start()

    def pushed(src, dst, send, recv, kk, tt):
        same = jnp.logical_and(kk == k, tt == t)

        @pl.when(jnp.logical_not(same))
        def _():
            remote(src, dst, send, recv, kk, tt).wait_send()

    def each(count, body):
        def step(i, carry):
            body(i)
            return carry

        lax.fori_loop(0, count, step, 0)

    def arrive(buffer, sems, count):
        each(
            count,
            lambda i: pltpu.make_async_copy(buffer.at[i], buffer.at[i], sems.at[i]).wait(),
        )

    for i in range(3):
        loads[i].wait()
    scaled = (tok[...].astype(F32) * tgain[...]).astype(BF16)
    query = jnp.dot(scaled, wq[...], preferred_element_type=F32)
    if query.shape[1] % LANES:
        pad = LANES - query.shape[1] % LANES
        query = jnp.concatenate([query, jnp.zeros((batch, pad), F32)], axis=1)
    for dest in range(kv):
        group, head = dest // per_row, (dest % per_row) % lh
        first = head * head_w // LANES * LANES
        q_send[dest] = query[group * seqs : (group + 1) * seqs, first : first + chunk]
    wide = scaled.astype(F32)
    for group in range(tp):
        scaled_s[group] = wide[group * seqs : (group + 1) * seqs]
    own = scaled_s[t].astype(BF16)
    loads[3].wait()
    loads[4].wait()
    lat = jnp.dot(own, wd[...], preferred_element_type=F32)
    rope = jnp.dot(own, wr[...], preferred_element_type=F32)
    for i in range(seqs):
        lat_send[i, :, :latent] = lat[i : i + 1]
        lat_send[i, :, latent:] = jnp.zeros((1, LANES), F32)
        lat_send[i, :, latent : latent + rope_w] = rope[i : i + 1]

    pl.semaphore_wait(barrier, kv * tp - 1)

    q_args = lambda i: (q_send.at[i], q_recv.at[k], q_ss.at[i], q_rs.at[k], i, t)
    lat_args = lambda i: (
        lat_send.at[i // lat_dup],
        lat_recv.at[k],
        lat_ss.at[i],
        lat_rs.at[k],
        i,
        t,
    )
    each(kv, lambda i: push(*q_args(i)))
    each(kv, lambda i: push(*lat_args(i)))

    group = k // per_row
    head = (k % per_row) % lh
    copy_at = (k % per_row) // lh
    for i in range(5, 8):
        loads[i].wait()
    arrive(q_recv, q_rs, kv)
    query = q_recv[0]
    for i in range(1, kv):
        query = query + q_recv[i]
    query = rounded(query)
    if lh > 1:
        shift = head * head_w % LANES
        query = jnp.where(shift == 0, query, pltpu.roll(query, chunk - head_w % LANES, 1))
    spun = rotated(query[:, nope_w : nope_w + LANES], cos[group], sin[group], half)
    ql_send[:, :latent] = dot_t(query[:, :nope_w].astype(BF16), wku[head]).astype(BF16)
    ql_send[:, latent:] = spun.astype(BF16)
    ql_args = lambda i: (
        ql_send,
        ql_recv.at[t * lh + head],
        ql_ss.at[i],
        ql_rs.at[t * lh + head],
        copy_at + dup * i,
        group,
    )
    each(kv // dup, lambda i: push(*ql_args(i)))

    loads[8].wait()
    arrive(lat_recv, lat_rs, kv)
    fresh = lat_recv[0]
    for i in range(1, kv):
        fresh = fresh + lat_recv[i]
    fresh_lat = fresh[:, :latent]
    scale = lax.rsqrt(jnp.mean(fresh_lat * fresh_lat, axis=1, keepdims=True) + EPSILON)
    seq = k // lat_dup
    pick = lax.broadcasted_iota(jnp.int32, (seqs, LANES), 0) == seq
    own_cos = jnp.sum(jnp.where(pick, cos[t], 0.0), axis=0, keepdims=True)
    own_sin = jnp.sum(jnp.where(pick, sin[t], 0.0), axis=0, keepdims=True)
    row_send[:, :latent] = rounded(fresh_lat * scale * lgain[...])
    row_send[:, latent:] = rounded(rotated(fresh[:, latent:], own_cos, own_sin, half))
    row_args = lambda i: (
        row_send,
        row_recv.at[seq],
        row_ss.at[i],
        row_rs.at[seq],
        k % lat_dup + lat_dup * i,
        t,
    )
    each(kv // lat_dup, lambda i: push(*row_args(i)))

    loads[9].wait()
    loads[10].wait()
    arrive(ql_recv, ql_rs, heads)
    for i in range(heads):
        wide = ql_recv[i].astype(F32)
        for c in range(full // LANES):
            q32[c, i * seqs : (i + 1) * seqs, :] = wide[:, c * LANES : (c + 1) * LANES]
    place = k * pos + lax.broadcasted_iota(jnp.int32, (heads, pos), 1)
    lane = lax.broadcasted_iota(jnp.int32, (heads, LANES), 1)
    all_scores = []
    for b in range(seqs):
        q_b = jnp.concatenate(
            [q32[c, pl.ds(b, heads, stride=seqs), :] for c in range(full // LANES)], axis=1
        ).astype(BF16)
        all_scores.append(
            (dot_t(q_b[:, :latent], cl[b]) + dot_t(q_b[:, latent : latent + rope_w], cr[b]))
            * factor
        )
    for b in range(seqs):
        visible = place < lengths[t * seqs + b]
        scores = jnp.where(visible, all_scores[b], NEGATIVE)
        top = jnp.max(scores, axis=1, keepdims=True)
        weights = jnp.where(visible, jnp.exp(scores - top), 0.0)
        total = jnp.sum(weights, axis=1, keepdims=True)
        acc = jnp.dot(weights.astype(BF16), cl[b], preferred_element_type=F32)
        stats = jnp.zeros((heads, LANES), F32)
        for at, value in ((0, top), (3, total)):
            for i in range(3):
                piece = rounded(value)
                stats = jnp.where(lane == at + i, piece, stats)
                value = value - piece
        for c in range(latent // LANES):
            stage[c, pl.ds(b, heads, stride=seqs), :] = acc[:, c * LANES : (c + 1) * LANES]
        stage[latent // LANES, pl.ds(b, heads, stride=seqs), :] = stats
    for dest in range(kv):
        for c in range(full // LANES):
            part_send[dest, :, c * LANES : (c + 1) * LANES] = stage[
                c, dest * rows : (dest + 1) * rows, :
            ].astype(BF16)
    part_args = lambda i: (part_send.at[i], part_recv.at[k], part_ss.at[i], part_rs.at[k], i, t)
    each(kv, lambda i: push(*part_args(i)))

    head_at = k // parts
    part_at = k % parts
    arrive(row_recv, row_rs, seqs)
    new_key = jnp.concatenate([row_recv[i] for i in range(seqs)], axis=0)
    own_query = ql_recv[head_at].astype(F32)

    def part_of(values):
        result = values[:rows]
        for i in range(1, parts):
            result = jnp.where(part_at == i, values[i * rows : (i + 1) * rows], result)
        return result

    new_key = part_of(new_key)
    own_query = part_of(own_query)
    new_score = jnp.sum(own_query * new_key, axis=1, keepdims=True) * factor
    arrive(part_recv, part_rs, kv)
    tops, sums, accs = [], [], []
    best = new_score
    for i in range(kv):
        stats = part_recv[i, :, latent:].astype(F32)
        top = stats[:, 0:1] + stats[:, 1:2] + stats[:, 2:3]
        tops.append(top)
        sums.append(stats[:, 3:4] + stats[:, 4:5] + stats[:, 5:6])
        best = jnp.maximum(best, top)
    new_weight = jnp.exp(new_score - best)
    weighted = rounded(new_weight) * new_key[:, :latent]
    weight_sum = new_weight
    for i in range(kv):
        share = jnp.exp(tops[i] - best)
        weight_sum = weight_sum + share * sums[i]
        weighted = weighted + share * part_recv[i, :, :latent].astype(F32)
    hl_send[...] = (weighted / weight_sum).astype(BF16)
    slot = (head_at % lh) * (tp * parts) + t * parts + part_at
    hl_args = lambda i: (
        hl_send,
        hl_recv.at[slot],
        hl_ss.at[i],
        hl_rs.at[slot],
        i,
        head_at // lh,
    )
    each(kv, lambda i: push(*hl_args(i)))

    for i in range(11, 14):
        loads[i].wait()
    arrive(hl_recv, hl_rs, lh * tp * parts)
    outs = []
    for i in range(lh):
        base = i * tp * parts
        block = jnp.concatenate(
            [hl_recv[base + j].astype(F32) for j in range(tp * parts)], axis=0
        ).astype(BF16)
        outs.append(jnp.dot(block, wvu[i], preferred_element_type=F32).astype(BF16))
    head_out = outs[0] if lh == 1 else jnp.concatenate(outs, axis=1)
    mix_send[...] = jnp.dot(head_out, wo[...], preferred_element_type=F32).astype(BF16)
    mix_args = lambda i: (mix_send, mix_recv.at[t], mix_ss.at[i], mix_rs.at[t], k, i)
    each(tp, lambda i: push(*mix_args(i)))
    arrive(mix_recv, mix_rs, tp)
    mixed = mix_recv[0].astype(F32)
    for i in range(1, tp):
        mixed = mixed + mix_recv[i].astype(F32)

    squares = jnp.sum(mixed * mixed, axis=1, keepdims=True)
    diagonal = lax.broadcasted_iota(jnp.int32, (batch, LANES), 0) == lax.broadcasted_iota(
        jnp.int32, (batch, LANES), 1
    )
    sq_send[...] = jnp.broadcast_to(
        jnp.sum(jnp.where(diagonal, squares, 0.0), axis=0, keepdims=True), sq_send.shape
    )
    sq_args = lambda i: (sq_send, sq_recv.at[k], sq_ss.at[i], sq_rs.at[k], i, t)
    each(kv, lambda i: push(*sq_args(i)))
    arrive(sq_recv, sq_rs, kv)
    line = sq_recv[0]
    for i in range(1, kv):
        line = line + sq_recv[i]
    squares = jnp.sum(jnp.where(diagonal, line[0:1], 0.0), axis=1, keepdims=True)
    out[...] = (mixed * lax.rsqrt(squares / model_w + EPSILON) * ogain[...]).astype(out.dtype)

    each(kv, lambda i: pushed(*q_args(i)))
    each(kv, lambda i: pushed(*lat_args(i)))
    each(kv // dup, lambda i: pushed(*ql_args(i)))
    each(kv // lat_dup, lambda i: pushed(*row_args(i)))
    each(kv, lambda i: pushed(*part_args(i)))
    each(kv, lambda i: pushed(*hl_args(i)))
    each(tp, lambda i: pushed(*mix_args(i)))
    each(kv, lambda i: pushed(*sq_args(i)))


def on_device(
    kv,
    tp,
    tokens,
    token_gain,
    w_query,
    w_down_kv,
    w_rope_key,
    latent_gain,
    w_key_up,
    w_value_up,
    w_out,
    out_gain,
    cache_latent,
    cache_rope,
    lengths,
):
    batch = tokens.shape[0]
    lh, latent, nope_w = w_key_up.shape
    rope_w = w_rope_key.shape[1]
    seqs = cache_latent.shape[0]
    heads = lh * tp
    full = latent + LANES
    rows = heads * seqs // kv
    per_row = kv // tp
    parts = seqs // rows
    assert kv % tp == 0 and per_row % lh == 0 and kv % seqs == 0
    assert seqs % rows == 0 and batch == seqs * tp and batch <= LANES
    dup = per_row // lh
    lat_dup = kv // seqs
    chunk = -(-(nope_w + rope_w) // LANES) * LANES

    inverse_freq = 1.0 / 10000.0 ** (jnp.arange(0, rope_w, 2, dtype=F32) / rope_w)
    angles = lengths.astype(F32)[:, None] * inverse_freq[None, :]
    cosine, sine = jnp.cos(angles), jnp.sin(angles)
    blank = jnp.zeros((batch, LANES - rope_w), F32)
    cos = jnp.concatenate([cosine, cosine, blank], axis=1).reshape(tp, seqs, LANES)
    sin = jnp.concatenate([-sine, sine, blank], axis=1).reshape(tp, seqs, LANES)

    arrays = [
        tokens,
        token_gain[None, :],
        w_query,
        w_down_kv,
        w_rope_key,
        cos,
        sin,
        w_key_up,
        cache_latent,
        cache_rope,
        latent_gain[None, :],
        w_value_up,
        w_out,
        out_gain[None, :],
    ]
    columns = w_out.shape[1]
    dma = lambda n: pltpu.SemaphoreType.DMA((n,))
    slots = lh * tp * parts
    return pl.pallas_call(
        functools.partial(kernel, kv, tp),
        out_shape=jax.ShapeDtypeStruct((batch, columns), BF16),
        in_specs=[pl.BlockSpec(memory_space=pltpu.SMEM)]
        + [pl.BlockSpec(memory_space=pl.ANY)] * len(arrays),
        out_specs=pl.BlockSpec(memory_space=pltpu.VMEM),
        scratch_shapes=[pltpu.VMEM(a.shape, a.dtype) for a in arrays]
        + [
            pltpu.VMEM((tp, seqs, tokens.shape[1]), F32),
            pltpu.VMEM((kv, seqs, chunk), F32),
            pltpu.VMEM((kv, seqs, chunk), F32),
            pltpu.VMEM((seqs, 1, full), F32),
            pltpu.VMEM((kv, 1, full), F32),
            pltpu.VMEM((1, full), F32),
            pltpu.VMEM((seqs, 1, full), F32),
            pltpu.VMEM((seqs, full), BF16),
            pltpu.VMEM((heads, seqs, full), BF16),
            pltpu.VMEM((full // LANES, heads * seqs, LANES), F32),
            pltpu.VMEM((full // LANES, heads * seqs, LANES), F32),
            pltpu.VMEM((kv, rows, full), BF16),
            pltpu.VMEM((kv, rows, full), BF16),
            pltpu.VMEM((rows, latent), BF16),
            pltpu.VMEM((slots, rows, latent), BF16),
            pltpu.VMEM((batch, columns), BF16),
            pltpu.VMEM((tp, batch, columns), BF16),
            pltpu.VMEM((8, LANES), F32),
            pltpu.VMEM((kv, 8, LANES), F32),
            dma(len(arrays)),
            dma(kv),
            dma(kv),
            dma(kv),
            dma(kv),
            dma(kv // lat_dup),
            dma(seqs),
            dma(kv // dup),
            dma(heads),
            dma(kv),
            dma(kv),
            dma(kv),
            dma(slots),
            dma(tp),
            dma(tp),
            dma(kv),
            dma(kv),
        ],
        compiler_params=pltpu.CompilerParams(
            collective_id=0, has_side_effects=True, vmem_limit_bytes=56 * 1024 * 1024
        ),
        name="decode",
    )(lengths, *arrays)


def solution(mesh):
    placed = (
        P(None, "kv"),
        P("kv"),
        P("kv", "tp"),
        P("kv", None),
        P("kv", None),
        P(),
        P("tp", None, None),
        P("tp", None, None),
        P("tp", "kv"),
        P("kv"),
        P("tp", "kv", None),
        P("tp", "kv", None),
        P(),
    )
    return jax.shard_map(
        functools.partial(on_device, mesh.shape["kv"], mesh.shape["tp"]),
        mesh=mesh,
        in_specs=placed,
        out_specs=P(None, "kv"),
        check_vma=False,
    )
```

time: 246 us -> 42 us (0.17)
  blocking collectives: 137 us -> 0 us
  waiting for transfers between devices: 59.7 us -> 0 us
  Pallas kernels: 0 us -> 34.7 us
  between operations: 13.6 us -> 0.02 us
  matrix products: 12.6 us -> 0 us
  other arithmetic: 12 us -> 1.51 us
  starting transfers between devices: 6.61 us -> 0 us
  local copies, waits for them, and re-layouts: 2.78 us -> 5.34 us
    psum x3 -> x0, blocking collectives: 69.7 us -> none  [the longest x1 39.4 us: on_device(): lax.psum((query_part, latent_part, rope_part), 'kv')]
    all_gather x2 -> x0, blocking collectives: 61.1 us -> none  [joined_2(): gathered = jax.tree.map(lambda a: lax.all_gather(a, axis), part)]
    psum x1 -> x0, waiting for transfers between devices: 55.9 us -> none  [on_device(): lax.psum((query_part, latent_part, rope_part), 'kv')]
    pallas_call x0 -> x1, Pallas kernels: none -> 34.7 us  [on_device(): pl.pallas_call(functools.partial(kernel, kv, tp), out_shape=jax.ShapeDtyp...]
    dot_general x11 -> x0, matrix products: 12.6 us -> none  [the longest x1 3.56 us: on_device(): jnp.einsum('bhl,blc->bhc', weights.astype(jnp.bfloat16), cache_latent, pr...]
    add x16 -> x0, other arithmetic: 7.13 us -> none  [the longest x7 7 us: combine_parts(): first_acc * first_fac[..., None] + second_acc * second_fac[..., None]]
    all_to_all x1 -> x0, blocking collectives: 6.67 us -> none  [on_device(): lax.all_to_all(head_latent, 'tp', split_axis=1, concat_axis=0, tiled=True)]
    all_to_all x2 -> x0, starting transfers between devices: 6.53 us -> none  [the longest x1 3.28 us: on_device(): lax.all_to_all(query_latent, 'tp', split_axis=0, concat_axis=1, tiled=True)]
  transfers between devices with their start and end apart: 4 -> 0, of which waited for: 2 -> 0; matrix products, arithmetic and copies ran while one was open for 4% -> 0% of each run, Pallas kernels for 0% -> 0%
where the time goes in v1:
time: 42 us; the launch traced here: 41.6 us
  Pallas kernels  34.7 us (83%)
  local copies, waits for them, and re-layouts  5.34 us (13%)
  other arithmetic  1.51 us (4%)
    pallas_call x1, Pallas kernels, on_device(): pl.pallas_call(functools.partial(kernel, kv, tp), out_shape=jax.ShapeDtyp...  34.7 us
    unnamed x3, local copies, waits for them, and re-layouts  5.18 us

profile of v1, /device:TPU:0, one launch (start us, length us, event | category | flops | bytes accessed | tf_op | source)
XLA Modules:
  0.0 41.6 jit_solution(6090112387403426367)
XLA Ops:
  0.0 0.7 %convert_element_type.3 = f32[32]{0:T(128)S(1)} convert(s32[32]{0:T(128)} %lengths.1) | non-fusion elementwise | flops 32 | bytes 256 | tf_op jit(solution)/shard_map/convert_element_type | solution.py:452
  0.7 0.1 pad.5.clone
  0.7 0.1 mul.22
  0.8 0.1 fusion
  1.0 0.7 %maximum_maximum_fusion.1 = (f32[4,8,128]{2,1,0:T(8,128)}, f32[4,8,128]{2,1,0:T(8,128)}) fusion(f32[4,8,32]{2,1,0:T(8,128)S(1)} %get-tuple-element.6, f32[4,8,32]{2,1,0:T(8,128)S(1)} %get-tuple-element.5, f32[128]{0:T(128)S(1)} %pad.5.clone, f32[4,8,32]{2,1,0:T(8,128)S(1)} %get-tuple-element.7), kind=kLoop, calls=%fused_computation.3 | loop fusion | flops 16384 | bytes 45568 | tf_op jit(solution)/shard_map/concatenate | solution.py:456
  1.7 1.5 %copy.14.wr_h = bf16[256,64]{1,0:T(8,128)(2,1)} copy(bf16[256,64]{0,1:T(8,128)(2,1)} %param.17) | data formatting | bytes 65536 | tf_op args[4]
  3.2 2.4 %copy.15.cr_h = bf16[8,512,64]{2,1,0:T(8,128)(2,1)} copy(bf16[8,512,64]{1,2,0:T(8,128)(2,1)} %param.24) | data formatting | bytes 1048576 | tf_op args[11]
  5.5 34.7 %decode.1 = bf16[32,256]{1,0:T(8,128)(2,1)} custom-call(s32[32]{0:T(128)} %lengths.1, bf16[32,256]{1,0:T(8,128)(2,1)} %tok_h.1, f32[1,256]{1,0:T(1,128)} %bitcast.4, bf16[256,384]{1,0:T(8,128)(2,1)} %wq_h.1, bf16[256,512]{1,0:T(8,128)(2,1)} %wd_h.1, bf16[256,64]{1,0:T(8,128)(2,1)} %copy.14.wr_h, f32[4,8,128]{2,1,0:T(8,128)} %get-tuple-element.9.cos_h, ...), custom_call_target="tpu_custom_call" | custom-call | tf_op jit(solution)/shard_map/decode/pallas_call | solution.py:477
  40.3 1.3 %copy.17 = bf16[32,256]{1,0:T(8,128)(2,1)} copy(bf16[32,256]{1,0:T(8,128)(2,1)} %decode.1) | data formatting | bytes 32768
  (2 shorter events, 0.0 us)

commit v2 on v1

--- a/solution.py
+++ b/solution.py
@@ -105,7 +105,7 @@
     t = lax.axis_index("tp")
     batch, width = tok.shape
     lh, latent, nope_w = wku.shape
-    rope_w = wr.shape[1]
+    rope_w = wr.shape[0]
     head_w = nope_w + rope_w
     half = rope_w // 2
     factor = head_w ** (-0.5)
@@ -217,7 +217,7 @@
     loads[3].wait()
     loads[4].wait()
     lat = jnp.dot(own, wd[...], preferred_element_type=F32)
-    rope = jnp.dot(own, wr[...], preferred_element_type=F32)
+    rope = dot_t(own, wr[...])
     for i in range(seqs):
         lat_send[i, :, :latent] = lat[i : i + 1]
         lat_send[i, :, latent:] = jnp.zeros((1, LANES), F32)
@@ -301,7 +301,12 @@
             [q32[c, pl.ds(b, heads, stride=seqs), :] for c in range(full // LANES)], axis=1
         ).astype(BF16)
         all_scores.append(
-            (dot_t(q_b[:, :latent], cl[b]) + dot_t(q_b[:, latent : latent + rope_w], cr[b]))
+            (
+                dot_t(q_b[:, :latent], cl[b])
+                + jnp.dot(
+                    q_b[:, latent : latent + rope_w], cr[b], preferred_element_type=F32
+                )
+            )
             * factor
         )
     for b in range(seqs):
@@ -460,12 +465,12 @@
         token_gain[None, :],
         w_query,
         w_down_kv,
-        w_rope_key,
+        w_rope_key.T,
         cos,
         sin,
         w_key_up,
         cache_latent,
-        cache_rope,
+        jnp.swapaxes(cache_rope, 1, 2),
         latent_gain[None, :],
         w_value_up,
         w_out,

time: 42 us -> 38 us (0.905)
  local copies, waits for them, and re-layouts: 5.34 us -> 1.48 us
    unnamed x3 -> x1, local copies, waits for them, and re-layouts: 5.18 us -> 1.32 us
where the time goes in v2:
time: 38 us; the launch traced here: 37.6 us
  Pallas kernels  34.6 us (91%)
  other arithmetic  1.5 us (4%)
  local copies, waits for them, and re-layouts  1.48 us (4%)
    pallas_call x1, Pallas kernels, on_device(): pl.pallas_call(functools.partial(kernel, kv, tp), out_shape=jax.ShapeDtyp...  34.6 us
    unnamed x1, local copies, waits for them, and re-layouts  1.32 us

profile of v2, /device:TPU:0, one launch (start us, length us, event | category | flops | bytes accessed | tf_op | source)
XLA Modules:
  0.0 37.6 jit_solution(715925640416760812)
XLA Ops:
  0.0 0.7 %convert_element_type.3 = f32[32]{0:T(128)S(1)} convert(s32[32]{0:T(128)} %lengths.1) | non-fusion elementwise | flops 32 | bytes 256 | tf_op jit(solution)/shard_map/convert_element_type | solution.py:457
  0.7 0.1 pad.5.clone
  0.7 0.1 mul.22
  0.8 0.1 fusion
  1.0 0.7 %maximum_maximum_fusion.1 = (f32[4,8,128]{2,1,0:T(8,128)}, f32[4,8,128]{2,1,0:T(8,128)}) fusion(f32[4,8,32]{2,1,0:T(8,128)S(1)} %get-tuple-element.6, f32[4,8,32]{2,1,0:T(8,128)S(1)} %get-tuple-element.5, f32[128]{0:T(128)S(1)} %pad.5.clone, f32[4,8,32]{2,1,0:T(8,128)S(1)} %get-tuple-element.7), kind=kLoop, calls=%fused_computation.3 | loop fusion | flops 16384 | bytes 45568 | tf_op jit(solution)/shard_map/concatenate | solution.py:461
  1.7 34.6 %decode.1 = bf16[32,256]{1,0:T(8,128)(2,1)} custom-call(s32[32]{0:T(128)} %lengths.1, bf16[32,256]{1,0:T(8,128)(2,1)} %tok_h.1, f32[1,256]{1,0:T(1,128)} %bitcast.8, bf16[256,384]{1,0:T(8,128)(2,1)} %wq_h.1, bf16[256,512]{1,0:T(8,128)(2,1)} %wd_h.1, bf16[64,256]{1,0:T(8,128)(2,1)} %bitcast.6, f32[4,8,128]{2,1,0:T(8,128)} %get-tuple-element.9.cos_h, ...), custom_call_target="tpu_custom_call" | custom-call | tf_op jit(solution)/shard_map/decode/pallas_call | solution.py:482
  36.3 1.3 %copy.15 = bf16[32,256]{1,0:T(8,128)(2,1)} copy(bf16[32,256]{1,0:T(8,128)(2,1)} %decode.1) | data formatting | bytes 32768
  (2 shorter events, 0.0 us)
